TPU v7x, 32 devices: a whole 2x2x4 slice. The times are simulated.
32 devices in a mesh: sp: 4 (over y, x), tp: 8 (over z, core).
Axes of the slice: x: 2, y: 2, z: 4, core: 2. Of those that a mesh axis runs over, the one named last changes fastest.
Arguments:
- prompt: bfloat16 [2, 8, 2, 4, 128, 2048], P(None, 'tp', None, 'sp'), may hold values from -60 to 60
- new_token: bfloat16 [2, 2048], replicated, may hold values from -20 to 20
- query_proj_matrix: bfloat16 [2048, 1024], P(None, 'tp'), may hold values from -1 to 1
- key_weight: bfloat16 [2048, 1024], P(None, 'tp'), may hold values from -1 to 1
- value_weight: bfloat16 [2048, 1024], P(None, 'tp'), may hold values from -0.125 to 0.125
- map_balance: float32 [8], replicated, may hold values from 0.3 to 0.8
- head_gain: float32 [128], replicated, may hold values from 0.1 to 1.9
Outputs:
- key_cache: bfloat16 [4, 8, 512, 1024], P('sp', 'tp')
- value_cache: bfloat16 [4, 8, 512, 1024], P('sp', 'tp')
- read: float32 [2, 1024], replicated
All inputs are finite; a program needn't handle non-finite values.
Results may differ from a plain program's by a relative error of at most 0.004.
The roundings to bfloat16 on the way count: a program that leaves them out, or rounds other values in their place, can miss the bound.
Values may be sent and summed in bfloat16 or wider, within the bound.
No kernel may reach another device: no remote copies, remote signals or barrier semaphores. Data moves between devices by JAX's collectives and lax.ppermute only.
A program may use at most 64 MiB of HBM per device.

v0:
```python
import jax
import jax.numpy as jnp
from jax import lax
from jax.sharding import PartitionSpec as P

HEADS = 8
MAP_HEAD_SIZE = 64
VD = 128


norm_eps = 1e-06
far_below = -1e30


def joined(part, axis, combine):
    gathered = jax.tree.map(lambda a: lax.all_gather(a, axis), part)

    def take(source):
        return jax.tree.map(lambda a: lax.dynamic_index_in_dim(a, source, 0, False), gathered)

    return lax.fori_loop(
        1, lax.axis_size(axis), lambda source, state: combine(state, take(source)), take(0)
    )


def fill_cols(source, w_piece):
    product = jnp.dot(source, w_piece, preferred_element_type=jnp.float32).astype(jnp.bfloat16)
    return product


def local_new(new_token, query_proj_matrix, key_weight, value_weight):
    return (
        jnp.dot(new_token, query_proj_matrix, preferred_element_type=jnp.float32).astype(
            jnp.bfloat16
        ),
        jnp.dot(new_token, key_weight, preferred_element_type=jnp.float32).astype(jnp.bfloat16),
        jnp.dot(new_token, value_weight, preferred_element_type=jnp.float32).astype(jnp.bfloat16),
    )


def partial_read(query_matrix_rows, key_rows, value_rows):
    logit_scores = jnp.einsum(
        "bhmd,bjhmd->bhmj", query_matrix_rows, key_rows, preferred_element_type=jnp.float32
    ) * MAP_HEAD_SIZE ** (-0.5)
    peak = jnp.max(logit_scores, axis=-1)
    weights_exp = jnp.exp(logit_scores - peak[..., None])
    totals = jnp.sum(weights_exp, axis=-1)
    weighted = jnp.einsum("bhmj,bjhe->bhme", weights_exp, value_rows.astype(jnp.float32))
    return (peak, totals, weighted)


def combine(first, second):
    peak_a, totals_a, weighted_a = first
    peak_b, totals_b, weighted_b = second
    peak = jnp.maximum(peak_a, peak_b)
    factor_a = jnp.exp(peak_a - peak)
    factor_b = jnp.exp(peak_b - peak)
    return (
        peak,
        totals_a * factor_a + totals_b * factor_b,
        weighted_a * factor_a[..., None] + weighted_b * factor_b[..., None],
    )


def shards(prompt, new_token, query_proj_matrix, key_weight, value_weight, map_balance, head_gain):
    seq_count, _, span_count, _, piece_rows, model_width = prompt.shape
    token_rows = prompt.reshape(seq_count * span_count * piece_rows, model_width)
    tp_count = lax.axis_size("tp")
    key_width = key_weight.shape[1] * tp_count
    value_width = value_weight.shape[1] * tp_count
    key_piece = lax.all_gather(key_weight, "tp", axis=1, tiled=True)
    value_piece = lax.all_gather(value_weight, "tp", axis=1, tiled=True)
    key_rows = fill_cols(token_rows, key_piece)
    value_rows = fill_cols(token_rows, value_piece)
    own_columns = local_new(new_token, query_proj_matrix, key_weight, value_weight)
    queries, new_keys, new_values = (
        lax.all_gather(own_columns[0], "tp", axis=1, tiled=True),
        lax.all_gather(own_columns[1], "tp", axis=1, tiled=True),
        lax.all_gather(own_columns[2], "tp", axis=1, tiled=True),
    )
    slot_count = seq_count * span_count
    cached_keys, cached_values = (
        lax.all_to_all(
            key_rows.reshape(slot_count, piece_rows, key_width),
            "sp",
            split_axis=0,
            concat_axis=1,
            tiled=True,
        ),
        lax.all_to_all(
            value_rows.reshape(slot_count, piece_rows, value_width),
            "sp",
            split_axis=0,
            concat_axis=1,
            tiled=True,
        ),
    )
    block_rows = cached_keys.shape[1]
    key_cache = cached_keys.reshape(1, 1, block_rows, key_width)
    value_cache = cached_values.reshape(1, 1, block_rows, value_width)
    all_queries = queries.reshape(seq_count, HEADS, 2, MAP_HEAD_SIZE)
    own_seq = lax.axis_index("sp") // span_count
    own_query = lax.dynamic_slice_in_dim(all_queries, own_seq, 1, 0)
    peak, totals, weighted = partial_read(
        own_query,
        cached_keys.reshape(1, block_rows, HEADS, 2, MAP_HEAD_SIZE),
        cached_values.reshape(1, block_rows, HEADS, VD),
    )
    chosen = jnp.arange(seq_count) == own_seq
    chosen_rows = chosen[:, None, None]
    spread = (
        jnp.where(chosen_rows, peak, far_below),
        jnp.where(chosen_rows, totals, 0.0),
        jnp.where(chosen_rows[..., None], weighted, 0.0),
    )
    merged = joined(spread, ("sp", "tp"), combine)
    own_keys = new_keys.reshape(seq_count, HEADS, 2, MAP_HEAD_SIZE)
    own_score = jnp.einsum(
        "bhmd,bhmd->bhm", all_queries, own_keys, preferred_element_type=jnp.float32
    ) * MAP_HEAD_SIZE ** (-0.5)
    own_values = new_values.astype(jnp.float32).reshape(seq_count, HEADS, VD)
    own_weighted = jnp.broadcast_to(own_values[:, :, None, :], (seq_count, HEADS, 2, VD))
    own_state = (own_score, jnp.ones_like(own_score), own_weighted)
    _, totals, weighted = combine(merged, own_state)
    heads_out = weighted / totals[..., None]
    blended = heads_out[:, :, 0] - map_balance[None, :, None] * heads_out[:, :, 1]
    normed = (
        blended
        * lax.rsqrt(jnp.mean(blended * blended, axis=-1, keepdims=True) + norm_eps)
        * head_gain
    )
    return (key_cache, value_cache, normed.reshape(seq_count, HEADS * VD))


def solution(mesh):
    in_specs = (
        P(None, "tp", None, "sp", None, None),
        P(),
        P(None, "tp"),
        P(None, "tp"),
        P(None, "tp"),
        P(),
        P(),
    )
    out_specs = (P("sp", "tp", None, None), P("sp", "tp", None, None), P())
    return jax.shard_map(shards, mesh=mesh, in_specs=in_specs, out_specs=out_specs, check_vma=False)
```

profile of v0, /device:TPU:0, one launch (start us, length us, event | category | flops | bytes accessed | tf_op | source)
XLA Modules:
  0.0 288.2 jit_solution(11000277364119802212)
XLA Ops:
  8.7 1.2 convolution_convert_fusion.4
  10.0 13.5 %all_gather.29 = bf16[2,1024]{1,0:T(2,128)(2,1)S(1)} all-gather(bf16[2,128]{1,0:T(2,128)(2,1)S(1)} %convolution_convert_fusion.4), channel_id=1, replica_groups=mesh['sp'=4,'tp'=8] {'tp'}, dimensions={1}, use_global_device_ids=true | all-gather | bytes 4608 | tf_op jit(solution)/shard_map/all_gather | solution.py:77
  23.5 1.2 convolution_convert_fusion.3
  24.7 9.2 %all_gather.33 = bf16[2,1024]{1,0:T(2,128)(2,1)S(1)} all-gather(bf16[2,128]{1,0:T(2,128)(2,1)S(1)} %convolution_convert_fusion.3), channel_id=1, replica_groups=mesh['sp'=4,'tp'=8] {'tp'}, dimensions={1}, use_global_device_ids=true | all-gather | bytes 4608 | tf_op jit(solution)/shard_map/all_gather | solution.py:78
  34.2 11.9 %all_gather.34 = bf16[2,1024]{1,0:T(2,128)(2,1)S(1)} all-gather(bf16[2,128]{1,0:T(2,128)(2,1)S(1)} %convolution_convert_fusion.2), channel_id=1, replica_groups=mesh['sp'=4,'tp'=8] {'tp'}, dimensions={1}, use_global_device_ids=true | all-gather | bytes 4608 | tf_op jit(solution)/shard_map/all_gather | solution.py:79
  46.3 14.0 %all-gather.3.cloned.1.call-done = bf16[2048,1024]{1,0:T(8,128)(2,1)} async-done(((bf16[2048,128]{1,0:T(8,128)(2,1)}), bf16[2048,1024]{1,0:T(8,128)(2,1)}) %all-gather.3.cloned.1.call-update) | async-done | bytes 4194320 | tf_op jit(solution)/shard_map/all_gather | solution.py:71
  60.2 4.5 %convolution_convert_fusion.1 = bf16[512,1024]{1,0:T(8,128)(2,1)S(1)} fusion(bf16[512,2048]{1,0:T(8,128)(2,1)S(1)} %bitcast.91, bf16[2048,1024]{1,0:T(8,128)(2,1)} %all-gather.3.cloned.1.call-done), kind=kOutput, calls=%fused_computation.11 | convolution fusion | flops 2148007936 | bytes 7340032 | tf_op jit(solution)/shard_map/dot_general | solution.py:27
  64.7 1.3 copy.43
  66.1 3.7 %all-to-all-start = ((bf16[4,128,1024]{1,2,0:T(8,128)(2,1)}), bf16[4,128,1024]{1,2,0:T(8,128)(2,1)S(1)}, u32[]{:S(2)}, u32[]{:S(2)}) async-start(bf16[4,128,1024]{1,2,0:T(8,128)(2,1)} %copy.43), calls=%async_computation | async-start | bytes 2097152 | tf_op jit(solution)/shard_map/all_to_all | solution.py:83
  69.8 38.0 %all-gather.5.cloned.1.call-done = bf16[2048,1024]{1,0:T(8,128)(2,1)} async-done(((bf16[2048,128]{1,0:T(8,128)(2,1)}), bf16[2048,1024]{1,0:T(8,128)(2,1)}) %all-gather.5.cloned.1.call-update) | async-done | bytes 4194320 | tf_op jit(solution)/shard_map/all_gather | solution.py:72
  107.8 5.5 %convolution_convert_fusion = bf16[512,1024]{1,0:T(8,128)(2,1)} fusion(bf16[512,2048]{1,0:T(8,128)(2,1)S(1)} %bitcast.92, bf16[2048,1024]{1,0:T(8,128)(2,1)} %all-gather.5.cloned.1.call-done), kind=kOutput, calls=%fused_computation.10 | convolution fusion | flops 2148007936 | bytes 7340032 | tf_op jit(solution)/shard_map/dot_general | solution.py:27
  113.3 4.2 %all-to-all-start.1 = ((bf16[4,128,1024]{2,1,0:T(8,128)(2,1)}), bf16[4,128,1024]{2,1,0:T(8,128)(2,1)}, u32[]{:S(2)}, u32[]{:S(2)}) async-start(bf16[4,128,1024]{2,1,0:T(8,128)(2,1)} %bitcast.93), calls=%async_computation.1 | async-start | bytes 2097152 | tf_op jit(solution)/shard_map/all_to_all | solution.py:90
  117.6 1.8 copy.45
  119.4 2.3 reshape.114
  121.6 1.5 fusion.11
  123.6 39.7 %all_gather.31 = f32[32,2,8,2]{2,3,1,0:T(2,128)S(1)} all-gather(f32[1,2,8,2]{2,3,1,0:T(2,128)S(1)} %get-tuple-element.222), channel_id=1, replica_groups=mesh['sp'=4,'tp'=8] {'sp','tp'}, dimensions={0}, use_global_device_ids=true | all-gather | bytes 4224 | tf_op jit(solution)/shard_map/all_gather | solution.py:16
  163.3 36.9 %all_gather.30 = f32[32,2,8,2]{2,3,1,0:T(2,128)S(1)} all-gather(f32[1,2,8,2]{2,3,1,0:T(2,128)S(1)} %get-tuple-element.223), channel_id=1, replica_groups=mesh['sp'=4,'tp'=8] {'sp','tp'}, dimensions={0}, use_global_device_ids=true | all-gather | bytes 4224 | tf_op jit(solution)/shard_map/all_gather | solution.py:16
  200.2 1.5 copy.66
  202.1 40.1 %all_gather.32 = f32[32,2,8,2,128]{4,2,3,1,0:T(8,128)S(1)} all-gather(f32[1,2,8,2,128]{4,2,3,1,0:T(8,128)S(1)} %broadcast_select_fusion), channel_id=1, replica_groups=mesh['sp'=4,'tp'=8] {'sp','tp'}, dimensions={0}, use_global_device_ids=true | all-gather | bytes 540672 | tf_op jit(solution)/shard_map/all_gather | solution.py:16
  242.2 0.8 copy-done.2
  243.0 33.5 %while.19 = (s32[]{:T(128)}, f32[2,8,2]{1,2,0:T(2,128)S(1)}, f32[2,8,2]{1,2,0:T(2,128)S(1)}, f32[2,8,2,128]{3,2,1,0:T(2,128)S(1)}, f32[32,2,8,2]{2,3,1,0:T(2,128...) while((s32[]{:T(128)}, f32[2,8,2]{1,2,0:T(2,128)S(1)}, ...), condition=%wide.region_3.4_spmd, body=%wide.region_2.3_spmd.sunk | while | flops 12485 | bytes 83855 | solution.py:21
  245.3 0.7 constant_dynamic-slice_fusion.2
  277.8 1.3 copy.44
  279.1 2.3 copy.112
  (203 shorter events, 36.4 us)
Async XLA Ops:
  7.2 53.1 %copy-start = (bf16[2,1,2,1,128,2048]{5,4,3,2,1,0:T(8,128)(2,1)S(1)}, bf16[2,1,2,1,128,2048]{5,4,3,2,1,0:T(8,128)(2,1)}, u32[]{:S(2)}) copy-start(bf16[2,1,2,1,128,2048]{5,4,3,2,1,0:T(8,128)(2,1)} %param.9) | copy-start | bytes 6291460
  7.2 26.8 %copy-start.1 = (bf16[2048,128]{1,0:T(8,128)(2,1)S(1)}, bf16[2048,128]{1,0:T(8,128)(2,1)}, u32[]{:S(2)}) copy-start(bf16[2048,128]{1,0:T(8,128)(2,1)} %param.13) | copy-start | bytes 1572868
  7.2 26.8 %copy-start.3 = (bf16[2,2048]{1,0:T(2,128)(2,1)S(1)}, bf16[2,2048]{1,0:T(2,128)(2,1)}, u32[]{:S(2)}) copy-start(bf16[2,2048]{1,0:T(2,128)(2,1)} %param.10) | copy-start | bytes 24580
  7.2 39.0 %copy-start.4 = (f32[8]{0:T(128)S(1)}, f32[8]{0:T(128)}, u32[]{:S(2)}) copy-start(f32[8]{0:T(128)} %param.14) | copy-start | bytes 100
  7.2 39.0 %copy-start.5 = (f32[128]{0:T(128)S(1)}, f32[128]{0:T(128)}, u32[]{:S(2)}) copy-start(f32[128]{0:T(128)} %param.15) | copy-start | bytes 1540
  7.2 53.0 %all-gather.3.cloned.1.call-start = ((), (), s32[]{:S(2)}) async-start(), calls=%async_computation.2 | async-start | bytes 4718592 | tf_op jit(solution)/shard_map/all_gather | solution.py:71
  8.0 99.9 %all-gather.5.cloned.1.call-start = ((), (), s32[]{:S(2)}) async-start(), calls=%async_computation.3 | async-start | bytes 4718592 | tf_op jit(solution)/shard_map/all_gather | solution.py:72
  66.1 47.3 %all-to-all-start = ((bf16[4,128,1024]{1,2,0:T(8,128)(2,1)}), bf16[4,128,1024]{1,2,0:T(8,128)(2,1)S(1)}, u32[]{:S(2)}, u32[]{:S(2)}) async-start(bf16[4,128,1024]{1,2,0:T(8,128)(2,1)} %copy.43), calls=%async_computation | async-start | bytes 2097152 | tf_op jit(solution)/shard_map/all_to_all | solution.py:83
  113.3 86.8 %all-to-all-start.1 = ((bf16[4,128,1024]{2,1,0:T(8,128)(2,1)}), bf16[4,128,1024]{2,1,0:T(8,128)(2,1)}, u32[]{:S(2)}, u32[]{:S(2)}) async-start(bf16[4,128,1024]{2,1,0:T(8,128)(2,1)} %bitcast.93), calls=%async_computation.1 | async-start | bytes 2097152 | tf_op jit(solution)/shard_map/all_to_all | solution.py:90
  242.2 0.8 copy-start.2
Sparse Core Ops, SparseCore 0:
  9.6 50.5 all-gather.2
  61.8 45.9 all-gather.4
where the time goes:
time: 291 us; the launch traced here: 288 us
  blocking collectives  151 us (52%)
  waiting for transfers between devices  53.4 us (18%)
  local copies, waits for them, and re-layouts  39.8 us (14%)
  matrix products  14.4 us (5%)
  between operations  14.2 us (5%)
  starting transfers between devices  7.97 us (3%)
  other arithmetic  6.61 us (2%)
    all_gather x3, blocking collectives, joined(): gathered = jax.tree.map(lambda a: lax.all_gather(a, axis), part)  117 us
    all_gather x1, waiting for transfers between devices, shards(): value_piece = lax.all_gather(value_weight, 'tp', axis=1, tiled=True)  38 us
    dynamic_slice x31, local copies, waits for them, and re-layouts, take(): lax.dynamic_index_in_dim(a, source, 0, False)  22.3 us
    all_gather x1, waiting for transfers between devices, shards(): key_piece = lax.all_gather(key_weight, 'tp', axis=1, tiled=True)  14 us
    all_gather x1, blocking collectives, shards(): lax.all_gather(own_columns[0], 'tp', axis=1, tiled=True)  13.5 us
    all_gather x1, blocking collectives, shards(): lax.all_gather(own_columns[2], 'tp', axis=1, tiled=True)  11.9 us
    dot_general x2, matrix products, fill_cols(): jnp.dot(source, w_piece, preferred_element_type=jnp.float32)  10 us
    all_gather x1, blocking collectives, shards(): lax.all_gather(own_columns[1], 'tp', axis=1, tiled=True)  9.21 us
  transfers between devices with their start and end apart: 4, of which 2 were waited for; matrix products, arithmetic and copies ran while one was open for 7% of the time, Pallas kernels for 0%

commit v1 on v0

v1 whole, which is shorter than its diff:
```python
import jax
import jax.numpy as jnp
from jax import lax
from jax.sharding import PartitionSpec as P

HEADS = 8
MAP_HEAD_SIZE = 64
VD = 128


norm_eps = 1e-06


def two_parts(values):
    high = lax.reduce_precision(values, 8, 7)
    return high.astype(jnp.bfloat16), (values - high).astype(jnp.bfloat16)


def project(source, weight):
    return jnp.dot(source, weight, preferred_element_type=jnp.float32).astype(jnp.bfloat16)


def joined(peak, totals, weighted, axis):
    top = jnp.max(peak, axis=axis, keepdims=True)
    factor = jnp.exp(peak - top)
    return (
        jnp.squeeze(top, axis),
        jnp.sum(totals * factor, axis=axis),
        jnp.sum(weighted * factor[..., None], axis=axis),
    )


def packed(peak, totals, weighted):
    lanes = peak.shape + (VD // 2,)
    return jnp.concatenate(
        [
            weighted,
            jnp.broadcast_to(peak[..., None], lanes),
            jnp.broadcast_to(totals[..., None], lanes),
        ],
        axis=-1,
    )


def unpacked(state):
    width = state.shape[-1] - VD
    return state[..., width], state[..., width + VD // 2], state[..., :width]


def own_read(keys, rows, queries, value_weight):
    tp_count = lax.axis_size("tp")
    map_count = 2 * HEADS
    key_width = keys.shape[1]
    of_map = jnp.arange(key_width) // MAP_HEAD_SIZE == jnp.arange(map_count)[:, None]
    spread = jnp.where(of_map, queries[None, :], jnp.zeros((), queries.dtype))
    scores = lax.dot_general(
        spread, keys, (((1,), (1,)), ((), ())), preferred_element_type=jnp.float32
    ) * MAP_HEAD_SIZE ** (-0.5)
    peak = jnp.max(scores, axis=-1)
    weights_exp = jnp.exp(scores - peak[:, None])
    totals = jnp.sum(weights_exp, axis=-1)
    high, low = two_parts(weights_exp)
    mixed = jnp.dot(
        jnp.concatenate([high, low]), rows, preferred_element_type=jnp.float32
    )
    mixed = mixed[:map_count] + mixed[map_count:]
    state = packed(peak, totals, mixed)
    width = value_weight.shape[1]
    heads_here = max(1, width // VD)
    repeats = max(1, VD // width)
    state = state.reshape(HEADS // heads_here, 1, heads_here * 2, state.shape[-1])
    state = jnp.broadcast_to(state, (state.shape[0], repeats) + state.shape[2:])
    state = state.reshape((tp_count,) + state.shape[2:])
    state = lax.all_to_all(state, "tp", 0, 0, tiled=True)
    peak, totals, mixed = joined(*unpacked(state), 0)
    mixed = mixed.reshape(heads_here, 2, -1)
    head_weight = value_weight.reshape(value_weight.shape[0], heads_here, width // heads_here)
    high, low = two_parts(mixed)
    weighted = jnp.einsum(
        "hmd,dhe->hme",
        jnp.concatenate([high, low], axis=1),
        head_weight,
        preferred_element_type=jnp.float32,
    )
    weighted = weighted[:, :2] + weighted[:, 2:]
    return peak, totals, weighted.reshape(heads_here * 2, -1)


def shards(prompt, new_token, query_proj_matrix, key_weight, value_weight, map_balance, head_gain):
    seq_count, _, span_count, _, piece_rows, model_width = prompt.shape
    tp_count = lax.axis_size("tp")
    slot_count = seq_count * span_count
    key_piece = lax.all_gather(key_weight, "tp", axis=1, tiled=True)
    key_width = key_piece.shape[1]
    value_piece = lax.all_gather(value_weight, "tp", axis=1, tiled=True)
    value_width = value_piece.shape[1]
    rows = lax.all_to_all(
        prompt.reshape(slot_count, piece_rows, model_width),
        "sp",
        split_axis=0,
        concat_axis=1,
        tiled=True,
    )
    rows = rows.reshape(-1, model_width)
    own_columns = jnp.stack(
        [project(new_token, w) for w in (query_proj_matrix, key_weight, value_weight)]
    )
    queries, new_keys, new_values = lax.all_gather(own_columns, "tp", axis=2, tiled=True)
    keys = project(rows, key_piece)
    own_seq = lax.axis_index("sp") // span_count
    peak, totals, weighted = own_read(
        keys, rows, lax.dynamic_index_in_dim(queries, own_seq, 0, False), value_weight
    )
    state = lax.all_gather(packed(peak, totals, weighted), "sp")
    state = state.reshape((seq_count, span_count) + state.shape[1:])
    peak, totals, weighted = joined(*unpacked(state), 1)
    state = lax.all_gather(packed(peak, totals, weighted), "tp")
    peak, totals, weighted = unpacked(state)
    heads_here = weighted.shape[2] // 2
    groups = HEADS // heads_here
    repeats = tp_count // groups
    peak, totals = (
        jnp.swapaxes(
            a.reshape(groups, repeats, seq_count, heads_here, 2)[:, 0], 0, 1
        ).reshape(seq_count, HEADS, 2)
        for a in (peak, totals)
    )
    weighted = weighted.reshape(groups, repeats, seq_count, heads_here, 2, -1)
    weighted = jnp.transpose(weighted, (2, 0, 3, 4, 1, 5)).reshape(seq_count, HEADS, 2, VD)
    own_score = jnp.sum(
        (queries.astype(jnp.float32) * new_keys.astype(jnp.float32)).reshape(
            seq_count, HEADS, 2, MAP_HEAD_SIZE
        ),
        axis=-1,
    ) * MAP_HEAD_SIZE ** (-0.5)
    own_values = new_values.astype(jnp.float32).reshape(seq_count, HEADS, 1, VD)
    top = jnp.maximum(peak, own_score)
    cached_factor = jnp.exp(peak - top)
    own_factor = jnp.exp(own_score - top)
    totals = totals * cached_factor + own_factor
    weighted = weighted * cached_factor[..., None] + own_values * own_factor[..., None]
    heads_out = weighted / totals[..., None]
    blended = heads_out[:, :, 0] - map_balance[None, :, None] * heads_out[:, :, 1]
    normed = (
        blended
        * lax.rsqrt(jnp.mean(blended * blended, axis=-1, keepdims=True) + norm_eps)
        * head_gain
    )
    read = normed.reshape(seq_count, HEADS * VD)
    late_rows, read = lax.optimization_barrier((rows, read))
    values = project(late_rows, value_piece)
    key_cache = keys.reshape(1, 1, -1, key_width)
    value_cache = values.reshape(1, 1, -1, value_width)
    return (key_cache, value_cache, read)


def solution(mesh):
    in_specs = (
        P(None, "tp", None, "sp", None, None),
        P(),
        P(None, "tp"),
        P(None, "tp"),
        P(None, "tp"),
        P(),
        P(),
    )
    out_specs = (P("sp", "tp", None, None), P("sp", "tp", None, None), P())
    return jax.shard_map(shards, mesh=mesh, in_specs=in_specs, out_specs=out_specs, check_vma=False)
```

time: 291 us -> 126 us (0.43)
  blocking collectives: 151 us -> 36.3 us
  local copies, waits for them, and re-layouts: 39.8 us -> 2.6 us
  waiting for transfers between devices: 53.4 us -> 48 us
  other arithmetic: 6.61 us -> 2.16 us
    all_gather x6 -> x3, blocking collectives: 151 us -> 36.3 us  [the longest x1 15.9 us: shards(): state = lax.all_gather(packed(peak, totals, weighted), 'tp')]
    all_gather x1, waiting for transfers between devices: 38 us -> 2.5 us  [shards(): value_piece = lax.all_gather(value_weight, 'tp', axis=1, tiled=True)]
    dynamic_slice x31 -> x1, local copies, waits for them, and re-layouts: 22.3 us -> 0.03 us  [shards(): lax.dynamic_index_in_dim(queries, own_seq, 0, False)]
    all_to_all x2, waiting for transfers between devices: 0.01 us -> 22 us  [the longest x1 11.9 us: own_read(): state = lax.all_to_all(state, 'tp', 0, 0, tiled=True)]
    all_gather x1, waiting for transfers between devices: 14 us -> 22 us  [shards(): key_piece = lax.all_gather(key_weight, 'tp', axis=1, tiled=True)]
    exp x64 -> x2, local copies, waits for them, and re-layouts: 5.54 us -> 0.01 us  [the longest x1 0.01 us: shards(): cached_factor = jnp.exp(peak - top)]
    add x63 -> x2, other arithmetic: 5.18 us -> 0.04 us  [the longest x1 0.02 us: own_read(): mixed = mixed[:map_count] + mixed[map_count:]]
    unnamed x16, local copies, waits for them, and re-layouts: 4.63 us -> 0.42 us
  transfers between devices with their start and end apart: 4 -> 4, of which waited for: 2 -> 4; matrix products, arithmetic and copies ran while one was open for 7% -> 10% of each run, Pallas kernels for 0% -> 0%
where the time goes in v1:
time: 126 us; the launch traced here: 125 us
  waiting for transfers between devices  48 us (38%)
  blocking collectives  36.3 us (29%)
  between operations  14.3 us (11%)
  matrix products  12.8 us (10%)
  starting transfers between devices  8.89 us (7%)
  local copies, waits for them, and re-layouts  2.6 us (2%)
  other arithmetic  2.16 us (2%)
    all_gather x1, waiting for transfers between devices, shards(): key_piece = lax.all_gather(key_weight, 'tp', axis=1, tiled=True)  22 us
    all_gather x1, blocking collectives, shards(): state = lax.all_gather(packed(peak, totals, weighted), 'tp')  15.9 us
    all_gather x1, blocking collectives, shards(): lax.all_gather(own_columns, 'tp', axis=2, tiled=True)  12.3 us
    all_to_all x1, waiting for transfers between devices, own_read(): state = lax.all_to_all(state, 'tp', 0, 0, tiled=True)  11.9 us
    dot_general x5, matrix products, project(): jnp.dot(source, weight, preferred_element_type=jnp.float32)  11.6 us
    all_to_all x1, waiting for transfers between devices, shards(): lax.all_to_all(prompt.reshape(slot_count, piece_rows, model_width), 'sp',...  10.1 us
    all_gather x1, blocking collectives, shards(): state = lax.all_gather(packed(peak, totals, weighted), 'sp')  8.06 us
    all_to_all x1, starting transfers between devices, shards(): lax.all_to_all(prompt.reshape(slot_count, piece_rows, model_width), 'sp',...  5.34 us
  transfers between devices with their start and end apart: 4, of which 4 were waited for; matrix products, arithmetic and copies ran while one was open for 10% of the time, Pallas kernels for 0%

profile of v1, /device:TPU:0, one launch (start us, length us, event | category | flops | bytes accessed | tf_op | source)
XLA Modules:
  0.0 124.9 jit_solution(4377040510684285517)
XLA Ops:
  7.2 0.7 all-gather.6.cloned.1.call-update
  7.9 5.3 %all-to-all-start = ((bf16[4,128,2048]{2,1,0:T(8,128)(2,1)}), bf16[4,128,2048]{2,1,0:T(8,128)(2,1)S(1)}, u32[]{:S(2)}, u32[]{:S(2)}) async-start(bf16[4,128,2048]{2,1,0:T(8,128)(2,1)} %bitcast.109), calls=%async_computation | async-start | bytes 4194304 | tf_op jit(solution)/shard_map/all_to_all | solution.py:97
  13.3 0.7 all-gather.8.cloned.1.call-update
  14.0 1.2 fusion.2
  15.3 0.2 fusion.3
  15.4 0.2 fusion.1
  15.7 12.3 %all_gather.22 = bf16[3,2,1024]{2,1,0:T(2,128)(2,1)S(1)} all-gather(bf16[3,2,128]{2,1,0:T(2,128)(2,1)S(1)} %pad_maximum_fusion.1), channel_id=1, replica_groups=mesh['sp'=4,'tp'=8] {'tp'}, dimensions={2}, use_global_device_ids=true | all-gather | bytes 13824 | tf_op jit(solution)/shard_map/all_gather | solution.py:108
  28.0 10.1 %all-to-all-done = bf16[4,128,2048]{2,1,0:T(8,128)(2,1)S(1)} async-done(((bf16[4,128,2048]{2,1,0:T(8,128)(2,1)}), bf16[4,128,2048]{2,1,0:T(8,128)(2,1)S(1)}, u32[]{:S(2)}, u32[]{:S(2)}) %all-to-all-start) | async-done | bytes 2097184 | tf_op jit(solution)/shard_map/all_to_all | solution.py:97
  38.1 22.0 %all-gather.6.cloned.1.call-done = bf16[2048,1024]{1,0:T(8,128)(2,1)} async-done(((bf16[2048,128]{1,0:T(8,128)(2,1)}), bf16[2048,1024]{1,0:T(8,128)(2,1)}) %all-gather.6.cloned.1.call-update) | async-done | bytes 4194320 | tf_op jit(solution)/shard_map/all_gather | solution.py:93
  60.2 4.5 %convolution_convert_fusion.1 = bf16[512,1024]{1,0:T(8,128)(2,1)S(1)} fusion(bf16[512,2048]{1,0:T(8,128)(2,1)S(1)} %bitcast.106, bf16[2048,1024]{1,0:T(8,128)(2,1)} %all-gather.6.cloned.1.call-done), kind=kOutput, calls=%fused_computation.1 | convolution fusion | flops 2148007936 | bytes 7340032 | tf_op jit(solution)/shard_map/dot_general | solution.py:20
  64.7 0.5 fusion.43
  65.2 0.2 fusion.13
  65.4 0.5 fusion.8
  66.2 0.7 reshape_reshape.3
  66.9 3.5 %all-to-all-start.1 = ((f32[8,2,2176]{2,1,0:T(2,128)}), f32[8,2,2176]{2,1,0:T(2,128)S(1)}, u32[]{:S(2)}, u32[]{:S(2)}) async-start(f32[8,2,2176]{2,1,0:T(2,128)} %reshape_reshape.3), calls=%async_computation.1 | async-start | bytes 278528 | tf_op jit(solution)/shard_map/all_to_all | solution.py:74
  70.7 11.9 %all-to-all-done.1 = f32[8,2,2176]{2,1,0:T(2,128)S(1)} async-done(((f32[8,2,2176]{2,1,0:T(2,128)}), f32[8,2,2176]{2,1,0:T(2,128)S(1)}, u32[]{:S(2)}, u32[]{:S(2)}) %all-to-all-start.1) | async-done | bytes 139296 | tf_op jit(solution)/shard_map/all_to_all | solution.py:74
  83.1 0.2 fusion.35
  83.4 0.2 convolution_bitcast_fusion
  83.8 8.1 %all-gather.2 = f32[4,2,256]{2,1,0:T(2,128)S(1)} all-gather(f32[1,2,256]{2,1,0:T(2,128)S(1)} %maximum_bitcast_fusion.2), channel_id=2, replica_groups=mesh['sp'=4,'tp'=8] {'sp'}, dimensions={0}, use_global_device_ids=true | all-gather | bytes 10240 | tf_op jit(solution)/shard_map/all_gather | solution.py:114
  92.6 15.9 %all-gather.1 = f32[16,2,256]{2,1,0:T(2,128)S(1)} all-gather(f32[2,2,256]{2,1,0:T(2,128)S(1)} %pad_maximum_fusion), channel_id=3, replica_groups=mesh['sp'=4,'tp'=8] {'tp'}, dimensions={0}, use_global_device_ids=true | all-gather | bytes 36864 | tf_op jit(solution)/shard_map/all_gather | solution.py:117
  109.1 0.2 multiply_reduce_fusion
  109.5 0.6 fusion.24
  110.1 2.5 %all-gather.8.cloned.1.call-done = bf16[2048,1024]{1,0:T(8,128)(2,1)} async-done(((bf16[2048,128]{1,0:T(8,128)(2,1)}), bf16[2048,1024]{1,0:T(8,128)(2,1)}) %all-gather.8.cloned.1.call-update) | async-done | bytes 4194320 | tf_op jit(solution)/shard_map/all_gather | solution.py:95
  112.6 5.5 %fusion = bf16[1,1,512,1024]{3,2,1,0:T(8,128)(2,1)} fusion(bf16[512,2048]{1,0:T(8,128)(2,1)S(1)} %bitcast.108, bf16[2048,1024]{1,0:T(8,128)(2,1)} %all-gather.8.cloned.1.call-done), kind=kOutput, calls=%fused_computation.2 | convolution fusion | flops 2148007936 | bytes 7340032 | tf_op jit(solution)/shard_map/dot_general | solution.py:20
  (60 shorter events, 2.9 us)
Async XLA Ops:
  7.2 8.3 %copy-start = (bf16[2048,128]{1,0:T(8,128)(2,1)S(1)}, bf16[2048,128]{1,0:T(8,128)(2,1)}, u32[]{:S(2)}) copy-start(bf16[2048,128]{1,0:T(8,128)(2,1)} %param.9) | copy-start | bytes 1572868
  7.2 53.0 %all-gather.6.cloned.1.call-start = ((), (), s32[]{:S(2)}) async-start(), calls=%async_computation.2 | async-start | bytes 4718592 | tf_op jit(solution)/shard_map/all_gather | solution.py:93
  7.9 6.1 %copy-start.3 = (bf16[2,2048]{1,0:T(2,128)(2,1)S(1)}, bf16[2,2048]{1,0:T(2,128)(2,1)}, u32[]{:S(2)}) copy-start(bf16[2,2048]{1,0:T(2,128)(2,1)} %param.8) | copy-start | bytes 24580
  7.9 7.3 %copy-start.1 = (bf16[2048,128]{1,0:T(8,128)(2,1)S(1)}, bf16[2048,128]{1,0:T(8,128)(2,1)}, u32[]{:S(2)}) copy-start(bf16[2048,128]{1,0:T(8,128)(2,1)} %param.11) | copy-start | bytes 1572868
  7.9 30.2 %all-to-all-start = ((bf16[4,128,2048]{2,1,0:T(8,128)(2,1)}), bf16[4,128,2048]{2,1,0:T(8,128)(2,1)S(1)}, u32[]{:S(2)}, u32[]{:S(2)}) async-start(bf16[4,128,2048]{2,1,0:T(8,128)(2,1)} %bitcast.109), calls=%async_computation | async-start | bytes 4194304 | tf_op jit(solution)/shard_map/all_to_all | solution.py:97
  13.3 99.3 %all-gather.8.cloned.1.call-start = ((), (), s32[]{:S(2)}) async-start(), calls=%async_computation.3 | async-start | bytes 4718592 | tf_op jit(solution)/shard_map/all_gather | solution.py:95
  64.7 1.2 copy-start.2
  65.2 5.4 %copy-start.4 = (f32[8]{0:T(128)S(1)}, f32[8]{0:T(128)}, u32[]{:S(2)}) copy-start(f32[8]{0:T(128)} %param.12) | copy-start | bytes 100
  65.2 5.4 %copy-start.5 = (f32[128]{0:T(128)S(1)}, f32[128]{0:T(128)}, u32[]{:S(2)}) copy-start(f32[128]{0:T(128)} %param.13) | copy-start | bytes 1540
  66.9 15.7 %all-to-all-start.1 = ((f32[8,2,2176]{2,1,0:T(2,128)}), f32[8,2,2176]{2,1,0:T(2,128)S(1)}, u32[]{:S(2)}, u32[]{:S(2)}) async-start(f32[8,2,2176]{2,1,0:T(2,128)} %reshape_reshape.3), calls=%async_computation.1 | async-start | bytes 278528 | tf_op jit(solution)/shard_map/all_to_all | solution.py:74
Sparse Core Ops, SparseCore 0:
  9.6 50.5 all-gather.5
  61.8 50.7 all-gather.7

commit v2 on v1

--- a/solution.py
+++ b/solution.py
@@ -1,6 +1,8 @@
 import jax
 import jax.numpy as jnp
 from jax import lax
+from jax.experimental import pallas as pl
+from jax.experimental.pallas import tpu as pltpu
 from jax.sharding import PartitionSpec as P
 
 HEADS = 8
@@ -18,6 +20,59 @@
 
 def project(source, weight):
     return jnp.dot(source, weight, preferred_element_type=jnp.float32).astype(jnp.bfloat16)
+
+
+def gathered(weight):
+    count = lax.axis_size("tp")
+    groups = [list(range(core, count, 2)) for core in range(2)]
+    return lax.all_gather(weight, "tp", axis=1, tiled=True, axis_index_groups=groups)
+
+
+def swapped(half):
+    count = lax.axis_size("tp")
+    return lax.ppermute(half, "tp", [(i, i ^ 1) for i in range(count)])
+
+
+def project_halves(rows, own, other, width):
+    first = (lax.axis_index("tp") % 2 == 0).astype(jnp.int32).reshape(1)
+    if width % 128:
+        even = jnp.where(first == 1, own, other)
+        odd = jnp.where(first == 1, other, own)
+        blocks = []
+        for start in range(0, own.shape[1], width):
+            blocks += [even[:, start : start + width], odd[:, start : start + width]]
+        return project(rows, jnp.concatenate(blocks, axis=1))
+
+    def kernel(first_ref, rows_ref, own_ref, other_ref, out_ref):
+        is_first = first_ref[0] == 1
+        mine, theirs = own_ref[...], other_ref[...]
+        pair = jnp.concatenate(
+            [jnp.where(is_first, mine, theirs), jnp.where(is_first, theirs, mine)], axis=1
+        )
+        out_ref[...] = jnp.dot(
+            rows_ref[...], pair, preferred_element_type=jnp.float32
+        ).astype(out_ref.dtype)
+
+    depth = rows.shape[1]
+    count = own.shape[1] // width
+    return pl.pallas_call(
+        kernel,
+        grid=(count,),
+        in_specs=[
+            pl.BlockSpec(memory_space=pltpu.SMEM),
+            pl.BlockSpec(rows.shape, lambda j: (0, 0)),
+            pl.BlockSpec((depth, width), lambda j: (0, j)),
+            pl.BlockSpec((depth, width), lambda j: (0, j)),
+        ],
+        out_specs=pl.BlockSpec((rows.shape[0], 2 * width), lambda j: (0, j)),
+        out_shape=jax.ShapeDtypeStruct((rows.shape[0], 2 * own.shape[1]), jnp.bfloat16),
+        cost_estimate=pl.CostEstimate(
+            flops=4 * rows.shape[0] * depth * own.shape[1],
+            transcendentals=0,
+            bytes_accessed=2 * (rows.size + 2 * own.size + 2 * rows.shape[0] * own.shape[1]),
+        ),
+        name="project_halves",
+    )(first, rows, own, other)
 
 
 def joined(peak, totals, weighted, axis):
@@ -90,10 +145,10 @@
     seq_count, _, span_count, _, piece_rows, model_width = prompt.shape
     tp_count = lax.axis_size("tp")
     slot_count = seq_count * span_count
-    key_piece = lax.all_gather(key_weight, "tp", axis=1, tiled=True)
-    key_width = key_piece.shape[1]
-    value_piece = lax.all_gather(value_weight, "tp", axis=1, tiled=True)
-    value_width = value_piece.shape[1]
+    key_width = key_weight.shape[1] * tp_count
+    value_width = value_weight.shape[1] * tp_count
+    key_half = gathered(key_weight)
+    value_half = gathered(value_weight)
     rows = lax.all_to_all(
         prompt.reshape(slot_count, piece_rows, model_width),
         "sp",
@@ -106,7 +161,8 @@
         [project(new_token, w) for w in (query_proj_matrix, key_weight, value_weight)]
     )
     queries, new_keys, new_values = lax.all_gather(own_columns, "tp", axis=2, tiled=True)
-    keys = project(rows, key_piece)
+    key_half, rows, queries = lax.optimization_barrier((key_half, rows, queries))
+    keys = project_halves(rows, key_half, swapped(key_half), key_weight.shape[1])
     own_seq = lax.axis_index("sp") // span_count
     peak, totals, weighted = own_read(
         keys, rows, lax.dynamic_index_in_dim(queries, own_seq, 0, False), value_weight
@@ -114,7 +170,10 @@
     state = lax.all_gather(packed(peak, totals, weighted), "sp")
     state = state.reshape((seq_count, span_count) + state.shape[1:])
     peak, totals, weighted = joined(*unpacked(state), 1)
-    state = lax.all_gather(packed(peak, totals, weighted), "tp")
+    state = packed(peak, totals, weighted)
+    value_half, state = lax.optimization_barrier((value_half, state))
+    other_values = swapped(value_half)
+    state = lax.all_gather(state, "tp")
     peak, totals, weighted = unpacked(state)
     heads_here = weighted.shape[2] // 2
     groups = HEADS // heads_here
@@ -148,7 +207,7 @@
     )
     read = normed.reshape(seq_count, HEADS * VD)
     late_rows, read = lax.optimization_barrier((rows, read))
-    values = project(late_rows, value_piece)
+    values = project_halves(late_rows, value_half, other_values, value_weight.shape[1])
     key_cache = keys.reshape(1, 1, -1, key_width)
     value_cache = values.reshape(1, 1, -1, value_width)
     return (key_cache, value_cache, read)

time: 126 us -> 137 us (1.087)
  blocking collectives: 36.3 us -> 51 us
  Pallas kernels: 0 us -> 12.6 us
  matrix products: 12.8 us -> 5.56 us
  waiting for transfers between devices: 48 us -> 43.4 us
  starting transfers between devices: 8.89 us -> 5.38 us
    all_to_all x0 -> x1, blocking collectives: none -> 16.5 us  [own_read(): state = lax.all_to_all(state, 'tp', 0, 0, tiled=True)]
    pallas_call x0 -> x2, Pallas kernels: none -> 12.6 us  [project_halves(): pl.pallas_call(kernel, grid=(count,), in_specs=[pl.BlockSpec(memory_space...]
    all_to_all x1 -> x0, waiting for transfers between devices: 11.9 us -> none  [own_read(): state = lax.all_to_all(state, 'tp', 0, 0, tiled=True)]
    dot_general x5 -> x3, matrix products: 11.6 us -> 1.59 us  [project(): jnp.dot(source, weight, preferred_element_type=jnp.float32)]
    ppermute x0 -> x2, waiting for transfers between devices: none -> 4.41 us  [swapped(): return lax.ppermute(half, 'tp', [(i, i ^ 1) for i in range(count)])]
    all_to_all x1 -> x0, starting transfers between devices: 3.51 us -> none  [own_read(): state = lax.all_to_all(state, 'tp', 0, 0, tiled=True)]
    all_gather x2, waiting for transfers between devices: 24.6 us -> 27.1 us  [gathered(): lax.all_gather(weight, 'tp', axis=1, tiled=True, axis_index_groups=groups)]
    dot_general x1, matrix products: 0.46 us -> 2.08 us  [own_read(): jnp.dot(jnp.concatenate([high, low]), rows, preferred_element_type=jnp.fl...]
  transfers between devices with their start and end apart: 4 -> 5, of which waited for: 4 -> 4; matrix products, arithmetic and copies ran while one was open for 10% -> 7% of each run, Pallas kernels for 0% -> 5%
where the time goes in v2:
time: 137 us; the launch traced here: 136 us
  blocking collectives  51 us (37%)
  waiting for transfers between devices  43.4 us (32%)
  between operations  14.3 us (10%)
  Pallas kernels  12.6 us (9%)
  matrix products  5.56 us (4%)
  starting transfers between devices  5.38 us (4%)
  other arithmetic  2.16 us (2%)
  local copies, waits for them, and re-layouts  1.95 us (1%)
    all_gather x2, waiting for transfers between devices, gathered(): lax.all_gather(weight, 'tp', axis=1, tiled=True, axis_index_groups=groups)  27.1 us
    all_to_all x1, blocking collectives, own_read(): state = lax.all_to_all(state, 'tp', 0, 0, tiled=True)  16.5 us
    all_gather x1, blocking collectives, shards(): state = lax.all_gather(state, 'tp')  14.4 us
    pallas_call x2, Pallas kernels, project_halves(): pl.pallas_call(kernel, grid=(count,), in_specs=[pl.BlockSpec(memory_space...  12.6 us
    all_gather x1, blocking collectives, shards(): lax.all_gather(own_columns, 'tp', axis=2, tiled=True)  12.1 us
    all_to_all x1, waiting for transfers between devices, shards(): lax.all_to_all(prompt.reshape(slot_count, piece_rows, model_width), 'sp',...  11.2 us
    all_gather x1, blocking collectives, shards(): state = lax.all_gather(packed(peak, totals, weighted), 'sp')  8 us
    all_to_all x1, starting transfers between devices, shards(): lax.all_to_all(prompt.reshape(slot_count, piece_rows, model_width), 'sp',...  5.34 us
  transfers between devices with their start and end apart: 5, of which 4 were waited for; matrix products, arithmetic and copies ran while one was open for 7% of the time, Pallas kernels for 5%

profile of v2, /device:TPU:0, one launch (start us, length us, event | category | flops | bytes accessed | tf_op | source)
XLA Modules:
  0.0 136.3 jit_solution(6397709689638076006)
XLA Ops:
  7.2 0.7 all-gather.6.cloned.1.call-update
  7.9 5.3 %all-to-all-start = ((bf16[4,128,2048]{2,1,0:T(8,128)(2,1)}), bf16[4,128,2048]{2,1,0:T(8,128)(2,1)S(1)}, u32[]{:S(2)}, u32[]{:S(2)}) async-start(bf16[4,128,2048]{2,1,0:T(8,128)(2,1)} %bitcast.112), calls=%async_computation | async-start | bytes 4194304 | tf_op jit(solution)/shard_map/all_to_all | solution.py:152
  13.3 1.2 fusion.1
  14.5 0.2 fusion
  14.7 0.2 fusion.2
  14.9 12.1 %all_gather.22 = bf16[3,2,1024]{2,1,0:T(2,128)(2,1)S(1)} all-gather(bf16[3,2,128]{2,1,0:T(2,128)(2,1)S(1)} %pad_maximum_fusion.1), channel_id=1, replica_groups=mesh['sp'=4,'tp'=8] {'tp'}, dimensions={2}, use_global_device_ids=true | all-gather | bytes 13824 | tf_op jit(solution)/shard_map/all_gather | solution.py:163
  27.0 11.2 %all-to-all-done = bf16[4,128,2048]{2,1,0:T(8,128)(2,1)S(1)} async-done(((bf16[4,128,2048]{2,1,0:T(8,128)(2,1)}), bf16[4,128,2048]{2,1,0:T(8,128)(2,1)S(1)}, u32[]{:S(2)}, u32[]{:S(2)}) %all-to-all-start) | async-done | bytes 2097184 | tf_op jit(solution)/shard_map/all_to_all | solution.py:152
  38.1 20.4 %all-gather.6.cloned.1.call-done.own_ref = bf16[2048,512]{1,0:T(8,128)(2,1)} async-done(((bf16[2048,128]{1,0:T(8,128)(2,1)}), bf16[2048,512]{1,0:T(8,128)(2,1)}) %all-gather.6.cloned.1.call-update) | async-done | bytes 2097168 | tf_op jit(solution)/shard_map/all_gather | solution.py:28
  58.6 4.4 %collective-permute-done.other_ref = bf16[2048,512]{1,0:T(8,128)(2,1)} collective-permute-done((bf16[2048,512]{1,0:T(8,128)(2,1)}, bf16[2048,512]{1,0:T(8,128)(2,1)}, u32[]{:S(2)}, u32[]{:S(2)}) %collective-permute-start) | collective-permute-done | bytes 2097184 | tf_op jit(solution)/shard_map/ppermute | solution.py:33
  63.0 6.4 %project_halves.2 = bf16[512,1024]{1,0:T(8,128)(2,1)} custom-call(s32[1]{0:T(128)} %bitcast.first_ref, bf16[512,2048]{1,0:T(8,128)(2,1)} %bitcast.109, bf16[2048,512]{1,0:T(8,128)(2,1)} %all-gather.6.cloned.1.call-done.own_ref, bf16[2048,512]{1,0:T(8,128)(2,1)} %collective-permute-done.other_ref), custom_call_target="tpu_custom_call" | custom-call | flops 2147483648 | bytes 7340032 | tf_op jit(solution)/shard_map/project_halves/pallas_call | solution.py:58
  69.4 1.7 %fusion.42 = (f32[16]{0:T(128)S(1)}, f32[16,512]{1,0:T(8,128)S(1)}) fusion(bf16[512,1024]{1,0:T(8,128)(2,1)} %project_halves.2, s32[1024]{0:T(1024)S(1)} %add_select_fusion, bf16[1024]{0:T(1024)(128)(2,1)S(1)} %dynamic-slice_reduce_fusion), kind=kOutput, calls=%fused_computation.83 | convolution fusion | flops 16826352 | bytes 1087552 | tf_op jit(solution)/shard_map/dot_general | solution.py:111
  71.1 0.2 fusion.12
  71.3 2.1 %fusion.7 = f32[32,2048]{1,0:T(8,128)S(1)} fusion(bf16[512,2048]{1,0:T(8,128)(2,1)} %bitcast.110, bf16[16,512]{1,0:T(8,128)(2,1)S(1)} %get-tuple-element.24, bf16[16,512]{1,0:T(8,128)(2,1)S(1)} %get-tuple-element.25), kind=kOutput, calls=%fused_computation.16 | convolution fusion | flops 67174400 | bytes 2392064 | tf_op jit(solution)/shard_map/dot_general | solution.py:118
  73.8 16.5 %all_to_all.14 = f32[8,2,2176]{2,1,0:T(2,128)S(1)} all-to-all(f32[8,2,2176]{2,1,0:T(2,128)S(1)} %reshape_reshape.3), channel_id=1, replica_groups=mesh['sp'=4,'tp'=8] {'tp'}, dimensions={0} | all-to-all | bytes 278528 | tf_op jit(solution)/shard_map/all_to_all | solution.py:129
  90.3 0.1 slice_reduce_fusion.1
  90.8 0.2 fusion.34
  91.0 0.1 fusion.3
  91.1 0.2 convolution_bitcast_fusion
  91.5 8.0 %all-gather.2 = f32[4,2,256]{2,1,0:T(2,128)S(1)} all-gather(f32[1,2,256]{2,1,0:T(2,128)S(1)} %maximum_bitcast_fusion.2), channel_id=2, replica_groups=mesh['sp'=4,'tp'=8] {'sp'}, dimensions={0}, use_global_device_ids=true | all-gather | bytes 10240 | tf_op jit(solution)/shard_map/all_gather | solution.py:170
  100.2 6.7 %all-gather.8.cloned.1.call-done.own_ref = bf16[2048,512]{1,0:T(8,128)(2,1)} async-done(((bf16[2048,128]{1,0:T(8,128)(2,1)}), bf16[2048,512]{1,0:T(8,128)(2,1)}) %all-gather.8.cloned.1.call-update) | async-done | bytes 2097168 | tf_op jit(solution)/shard_map/all_gather | solution.py:28
  107.2 14.4 %all-gather.1 = f32[16,2,256]{2,1,0:T(2,128)S(1)} all-gather(f32[2,2,256]{2,1,0:T(2,128)S(1)} %pad_maximum_fusion), channel_id=3, replica_groups=mesh['sp'=4,'tp'=8] {'tp'}, dimensions={0}, use_global_device_ids=true | all-gather | bytes 36864 | tf_op jit(solution)/shard_map/all_gather | solution.py:176
  122.3 0.2 multiply_reduce_fusion
  122.6 0.6 fusion.23
  123.2 6.3 %project_halves.3 = bf16[512,1024]{1,0:T(8,128)(2,1)} custom-call(s32[1]{0:T(128)} %bitcast.first_ref, bf16[512,2048]{1,0:T(8,128)(2,1)} %bitcast.111, bf16[2048,512]{1,0:T(8,128)(2,1)} %all-gather.8.cloned.1.call-done.own_ref, bf16[2048,512]{1,0:T(8,128)(2,1)} %collective-permute-done.1.other_ref), custom_call_target="tpu_custom_call" | custom-call | flops 2147483648 | bytes 7340032 | tf_op jit(solution)/shard_map/project_halves/pallas_call | solution.py:58
  (65 shorter events, 2.8 us)
Async XLA Ops:
  7.2 7.3 %copy-start = (bf16[2048,128]{1,0:T(8,128)(2,1)S(1)}, bf16[2048,128]{1,0:T(8,128)(2,1)}, u32[]{:S(2)}) copy-start(bf16[2048,128]{1,0:T(8,128)(2,1)} %param.9) | copy-start | bytes 1572868
  7.2 51.4 %all-gather.6.cloned.1.call-start = ((), (), s32[]{:S(2)}) async-start(), calls=%async_computation.2 | async-start | bytes 2621440 | tf_op jit(solution)/shard_map/all_gather | solution.py:28
  7.9 5.4 %copy-start.4 = (bf16[2,2048]{1,0:T(2,128)(2,1)S(1)}, bf16[2,2048]{1,0:T(2,128)(2,1)}, u32[]{:S(2)}) copy-start(bf16[2,2048]{1,0:T(2,128)(2,1)} %param.8) | copy-start | bytes 24580
  7.9 6.8 %copy-start.2 = (bf16[2048,128]{1,0:T(8,128)(2,1)S(1)}, bf16[2048,128]{1,0:T(8,128)(2,1)}, u32[]{:S(2)}) copy-start(bf16[2048,128]{1,0:T(8,128)(2,1)} %param.11) | copy-start | bytes 1572868
  7.9 30.2 %all-to-all-start = ((bf16[4,128,2048]{2,1,0:T(8,128)(2,1)}), bf16[4,128,2048]{2,1,0:T(8,128)(2,1)S(1)}, u32[]{:S(2)}, u32[]{:S(2)}) async-start(bf16[4,128,2048]{2,1,0:T(8,128)(2,1)} %bitcast.112), calls=%async_computation | async-start | bytes 4194304 | tf_op jit(solution)/shard_map/all_to_all | solution.py:152
  13.3 93.7 %all-gather.8.cloned.1.call-start = ((), (), s32[]{:S(2)}) async-start(), calls=%async_computation.3 | async-start | bytes 2621440 | tf_op jit(solution)/shard_map/all_gather | solution.py:28
  38.1 24.9 %copy-start.1 = (bf16[4,128,2048]{2,1,0:T(8,128)(2,1)}, bf16[4,128,2048]{2,1,0:T(8,128)(2,1)S(1)}, u32[]{:S(2)}) copy-start(bf16[4,128,2048]{2,1,0:T(8,128)(2,1)S(1)} %all-to-all-done) | copy-start | bytes 6291460
  58.5 4.5 %collective-permute-start = (bf16[2048,512]{1,0:T(8,128)(2,1)}, bf16[2048,512]{1,0:T(8,128)(2,1)}, u32[]{:S(2)}, u32[]{:S(2)}) collective-permute-start(bf16[2048,512]{1,0:T(8,128)(2,1)} %all-gather.6.cloned.1.call-done.own_ref), channel_id=1, source_target_pairs={{0,1},{1,0},{2,3},{3,2},{4,5},{5,4},{6,7},{7,6},{8,9},{9,8},{10,11... | collective-permute-start | bytes 6291464 | tf_op jit(solution)/shard_map/ppermute | solution.py:33
  71.1 20.0 %copy-start.3 = (bf16[2048,128]{1,0:T(8,128)(2,1)S(1)}, bf16[2048,128]{1,0:T(8,128)(2,1)}, u32[]{:S(2)}) copy-start(bf16[2048,128]{1,0:T(8,128)(2,1)} %param.11) | copy-start | bytes 1572868
  71.3 35.6 %copy-start.5 = (f32[8]{0:T(128)S(1)}, f32[8]{0:T(128)}, u32[]{:S(2)}) copy-start(f32[8]{0:T(128)} %param.12) | copy-start | bytes 100
  71.3 35.6 %copy-start.6 = (f32[128]{0:T(128)S(1)}, f32[128]{0:T(128)}, u32[]{:S(2)}) copy-start(f32[128]{0:T(128)} %param.13) | copy-start | bytes 1540
  106.9 16.3 %collective-permute-start.1 = (bf16[2048,512]{1,0:T(8,128)(2,1)}, bf16[2048,512]{1,0:T(8,128)(2,1)}, u32[]{:S(2)}, u32[]{:S(2)}) collective-permute-start(bf16[2048,512]{1,0:T(8,128)(2,1)} %all-gather.8.cloned.1.call-done.own_ref), channel_id=1, source_target_pairs={{0,1},{1,0},{2,3},{3,2},{4,5},{5,4},{6,7},{7,6},{8,9},{9,8},{10,11... | collective-permute-start | bytes 6291464 | tf_op jit(solution)/shard_map/ppermute | solution.py:33
Sparse Core Ops, SparseCore 0:
  9.5 48.9 all-gather.5
  60.1 46.7 all-gather.7

commit v3 on v1

--- a/solution.py
+++ b/solution.py
@@ -1,6 +1,7 @@
 import jax
 import jax.numpy as jnp
 from jax import lax
+from jax.experimental import pallas as pl
 from jax.sharding import PartitionSpec as P
 
 HEADS = 8
@@ -18,6 +19,47 @@
 
 def project(source, weight):
     return jnp.dot(source, weight, preferred_element_type=jnp.float32).astype(jnp.bfloat16)
+
+
+def gathered(weight):
+    count = lax.axis_size("sp")
+    part = weight.shape[0] // count
+    own = lax.dynamic_slice_in_dim(weight, lax.axis_index("sp") * part, part, 0)
+    whole = lax.all_gather(own, ("sp", "tp"), axis=0, tiled=True)
+    return whole.reshape(count, lax.axis_size("tp"), part, weight.shape[1])
+
+
+def project_blocks(rows, blocks):
+    parts, count, part, width = blocks.shape
+    depth = parts * part
+    if width % 128 or count % 2:
+        weight = jnp.transpose(blocks, (0, 2, 1, 3)).reshape(depth, count * width)
+        return project(rows, weight)
+
+    def kernel(rows_ref, block_ref, out_ref):
+        pair = jnp.concatenate(
+            [block_ref[:, side].reshape(depth, width) for side in range(2)], axis=1
+        )
+        out_ref[...] = jnp.dot(
+            rows_ref[...], pair, preferred_element_type=jnp.float32
+        ).astype(out_ref.dtype)
+
+    return pl.pallas_call(
+        kernel,
+        grid=(count // 2,),
+        in_specs=[
+            pl.BlockSpec(rows.shape, lambda j: (0, 0)),
+            pl.BlockSpec((parts, 2, part, width), lambda j: (0, j, 0, 0)),
+        ],
+        out_specs=pl.BlockSpec((rows.shape[0], 2 * width), lambda j: (0, j)),
+        out_shape=jax.ShapeDtypeStruct((rows.shape[0], count * width), jnp.bfloat16),
+        cost_estimate=pl.CostEstimate(
+            flops=2 * rows.shape[0] * blocks.size,
+            transcendentals=0,
+            bytes_accessed=2 * (rows.size + blocks.size + rows.shape[0] * count * width),
+        ),
+        name="project_blocks",
+    )(rows, blocks)
 
 
 def joined(peak, totals, weighted, axis):
@@ -90,10 +132,10 @@
     seq_count, _, span_count, _, piece_rows, model_width = prompt.shape
     tp_count = lax.axis_size("tp")
     slot_count = seq_count * span_count
-    key_piece = lax.all_gather(key_weight, "tp", axis=1, tiled=True)
-    key_width = key_piece.shape[1]
-    value_piece = lax.all_gather(value_weight, "tp", axis=1, tiled=True)
-    value_width = value_piece.shape[1]
+    key_width = key_weight.shape[1] * tp_count
+    value_width = value_weight.shape[1] * tp_count
+    key_blocks = gathered(key_weight)
+    value_blocks = gathered(value_weight)
     rows = lax.all_to_all(
         prompt.reshape(slot_count, piece_rows, model_width),
         "sp",
@@ -106,7 +148,7 @@
         [project(new_token, w) for w in (query_proj_matrix, key_weight, value_weight)]
     )
     queries, new_keys, new_values = lax.all_gather(own_columns, "tp", axis=2, tiled=True)
-    keys = project(rows, key_piece)
+    keys = project_blocks(rows, key_blocks)
     own_seq = lax.axis_index("sp") // span_count
     peak, totals, weighted = own_read(
         keys, rows, lax.dynamic_index_in_dim(queries, own_seq, 0, False), value_weight
@@ -114,7 +156,11 @@
     state = lax.all_gather(packed(peak, totals, weighted), "sp")
     state = state.reshape((seq_count, span_count) + state.shape[1:])
     peak, totals, weighted = joined(*unpacked(state), 1)
-    state = lax.all_gather(packed(peak, totals, weighted), "tp")
+    state = packed(peak, totals, weighted)
+    late_rows, state = lax.optimization_barrier((rows, state))
+    state = lax.all_to_all(
+        jnp.broadcast_to(state[None], (tp_count,) + state.shape), "tp", 0, 0, tiled=True
+    )
     peak, totals, weighted = unpacked(state)
     heads_here = weighted.shape[2] // 2
     groups = HEADS // heads_here
@@ -147,8 +193,7 @@
         * head_gain
     )
     read = normed.reshape(seq_count, HEADS * VD)
-    late_rows, read = lax.optimization_barrier((rows, read))
-    values = project(late_rows, value_piece)
+    values = project_blocks(late_rows, value_blocks)
     key_cache = keys.reshape(1, 1, -1, key_width)
     value_cache = values.reshape(1, 1, -1, value_width)
     return (key_cache, value_cache, read)

time: 126 us -> 160 us (1.27)
  waiting for transfers between devices: 48 us -> 87 us
  blocking collectives: 36.3 us -> 20.2 us
  Pallas kernels: 0 us -> 12.4 us
  matrix products: 12.8 us -> 5.59 us
  starting transfers between devices: 8.89 us -> 12.1 us
  local copies, waits for them, and re-layouts: 2.6 us -> 5.5 us
    all_gather x2, waiting for transfers between devices: 24.6 us -> 67 us  [gathered(): whole = lax.all_gather(own, ('sp', 'tp'), axis=0, tiled=True)]
    all_gather x1 -> x0, blocking collectives: 15.9 us -> none  [shards(): state = lax.all_gather(packed(peak, totals, weighted), 'tp')]
    pallas_call x0 -> x2, Pallas kernels: none -> 12.4 us  [project_blocks(): pl.pallas_call(kernel, grid=(count // 2,), in_specs=[pl.BlockSpec(rows.sh...]
    dot_general x5 -> x3, matrix products: 11.6 us -> 1.59 us  [project(): jnp.dot(source, weight, preferred_element_type=jnp.float32)]
    all_to_all x1, waiting for transfers between devices: 11.9 us -> 7.86 us  [own_read(): state = lax.all_to_all(state, 'tp', 0, 0, tiled=True)]
    all_to_all x0 -> x1, starting transfers between devices: none -> 3.34 us  [shards(): lax.all_to_all(jnp.broadcast_to(state[None], (tp_count,) + state.shape),...]
    dynamic_slice x0 -> x2, local copies, waits for them, and re-layouts: none -> 2.28 us  [gathered(): own = lax.dynamic_slice_in_dim(weight, lax.axis_index('sp') * part, part, 0)]
    all_to_all x1, waiting for transfers between devices: 10.1 us -> 12.1 us  [shards(): lax.all_to_all(prompt.reshape(slot_count, piece_rows, model_width), 'sp',...]
  transfers between devices with their start and end apart: 4 -> 5, of which waited for: 4 -> 4; matrix products, arithmetic and copies ran while one was open for 10% -> 6% of each run, Pallas kernels for 0% -> 8%
where the time goes in v3:
time: 160 us; the launch traced here: 159 us
  waiting for transfers between devices  87 us (54%)
  blocking collectives  20.2 us (13%)
  between operations  14.2 us (9%)
  Pallas kernels  12.4 us (8%)
  starting transfers between devices  12.1 us (8%)
  matrix products  5.59 us (3%)
  local copies, waits for them, and re-layouts  5.5 us (3%)
  other arithmetic  2.17 us (1%)
    all_gather x2, waiting for transfers between devices, gathered(): whole = lax.all_gather(own, ('sp', 'tp'), axis=0, tiled=True)  67 us
    pallas_call x2, Pallas kernels, project_blocks(): pl.pallas_call(kernel, grid=(count // 2,), in_specs=[pl.BlockSpec(rows.sh...  12.4 us
    all_to_all x1, waiting for transfers between devices, shards(): lax.all_to_all(prompt.reshape(slot_count, piece_rows, model_width), 'sp',...  12.1 us
    all_gather x1, blocking collectives, shards(): lax.all_gather(own_columns, 'tp', axis=2, tiled=True)  12 us
    all_gather x1, blocking collectives, shards(): state = lax.all_gather(packed(peak, totals, weighted), 'sp')  8.12 us
    all_to_all x1, waiting for transfers between devices, own_read(): state = lax.all_to_all(state, 'tp', 0, 0, tiled=True)  7.86 us
    all_to_all x1, starting transfers between devices, shards(): lax.all_to_all(prompt.reshape(slot_count, piece_rows, model_width), 'sp',...  5.34 us
    all_to_all x1, starting transfers between devices, own_read(): state = lax.all_to_all(state, 'tp', 0, 0, tiled=True)  3.37 us
  transfers between devices with their start and end apart: 5, of which 4 were waited for; matrix products, arithmetic and copies ran while one was open for 6% of the time, Pallas kernels for 8%

profile of v3, /device:TPU:0, one launch (start us, length us, event | category | flops | bytes accessed | tf_op | source)
XLA Modules:
  0.0 159.2 jit_solution(18019581121598126552)
XLA Ops:
  7.2 1.6 %constant_dynamic-slice_fusion.1 = bf16[512,128]{1,0:T(8,128)(2,1)} fusion(bf16[2048,128]{1,0:T(8,128)(2,1)} %param.10, s32[]{:T(128)S(6)} %select_n.26), kind=kLoop, calls=%fused_computation.75 | loop fusion | bytes 262148 | tf_op jit(solution)/shard_map/dynamic_slice | solution.py:27
  8.9 0.7 constant_dynamic-slice_fusion
  9.7 5.3 %all-to-all-start = ((bf16[4,128,2048]{2,1,0:T(8,128)(2,1)}), bf16[4,128,2048]{2,1,0:T(8,128)(2,1)S(1)}, u32[]{:S(2)}, u32[]{:S(2)}) async-start(bf16[4,128,2048]{2,1,0:T(8,128)(2,1)} %bitcast.105), calls=%async_computation | async-start | bytes 4194304 | tf_op jit(solution)/shard_map/all_to_all | solution.py:139
  15.0 0.2 fusion.1
  15.2 0.2 fusion.2
  15.4 1.2 fusion
  16.6 12.0 %all_gather.16 = bf16[3,2,1024]{2,1,0:T(2,128)(2,1)S(1)} all-gather(bf16[3,2,128]{2,1,0:T(2,128)(2,1)S(1)} %pad_maximum_fusion.1), channel_id=1, replica_groups=mesh['sp'=4,'tp'=8] {'tp'}, dimensions={2}, use_global_device_ids=true | all-gather | bytes 13824 | tf_op jit(solution)/shard_map/all_gather | solution.py:150
  28.7 12.1 %all-to-all-done = bf16[4,128,2048]{2,1,0:T(8,128)(2,1)S(1)} async-done(((bf16[4,128,2048]{2,1,0:T(8,128)(2,1)}), bf16[4,128,2048]{2,1,0:T(8,128)(2,1)S(1)}, u32[]{:S(2)}, u32[]{:S(2)}) %all-to-all-start) | async-done | bytes 2097184 | tf_op jit(solution)/shard_map/all_to_all | solution.py:139
  40.8 39.0 %all-gather.5.cloned.1.call-done = bf16[16384,128]{1,0:T(8,128)(2,1)} async-done(((bf16[512,128]{1,0:T(8,128)(2,1)}), bf16[16384,128]{1,0:T(8,128)(2,1)}) %all-gather.5.cloned.1.call-update) | async-done | bytes 4194320 | tf_op jit(solution)/shard_map/all_gather | solution.py:28
  79.8 6.2 %project_blocks.2 = bf16[512,1024]{1,0:T(8,128)(2,1)} custom-call(bf16[512,2048]{1,0:T(8,128)(2,1)} %bitcast.102, bf16[4,8,512,128]{3,2,1,0:T(8,128)(2,1)} %bitcast.116), custom_call_target="tpu_custom_call" | custom-call | flops 2147483648 | bytes 7340032 | tf_op jit(solution)/shard_map/project_blocks/pallas_call | solution.py:47
  86.0 1.7 %fusion.42 = (f32[16]{0:T(128)S(1)}, f32[16,512]{1,0:T(8,128)S(1)}) fusion(bf16[512,1024]{1,0:T(8,128)(2,1)} %project_blocks.2, s32[1024]{0:T(1024)S(1)} %add_select_fusion, bf16[1024]{0:T(1024)(128)(2,1)S(1)} %dynamic-slice_reduce_fusion), kind=kOutput, calls=%fused_computation.83 | convolution fusion | flops 16826352 | bytes 1087552 | tf_op jit(solution)/shard_map/dot_general | solution.py:98
  87.7 0.2 fusion.12
  87.9 2.1 %fusion.7 = f32[32,2048]{1,0:T(8,128)S(1)} fusion(bf16[512,2048]{1,0:T(8,128)(2,1)} %bitcast.103, bf16[16,512]{1,0:T(8,128)(2,1)S(1)} %get-tuple-element.14, bf16[16,512]{1,0:T(8,128)(2,1)S(1)} %get-tuple-element.15), kind=kOutput, calls=%fused_computation.16 | convolution fusion | flops 67174400 | bytes 2392064 | tf_op jit(solution)/shard_map/dot_general | solution.py:105
  90.3 0.7 reshape_reshape.3
  91.0 3.4 %all-to-all-start.1 = ((f32[8,2,2176]{2,1,0:T(2,128)}), f32[8,2,2176]{2,1,0:T(2,128)S(1)}, u32[]{:S(2)}, u32[]{:S(2)}) async-start(f32[8,2,2176]{2,1,0:T(2,128)} %reshape_reshape.3), calls=%async_computation.1 | async-start | bytes 278528 | tf_op jit(solution)/shard_map/all_to_all | solution.py:116
  94.7 7.9 %all-to-all-done.1 = f32[8,2,2176]{2,1,0:T(2,128)S(1)} async-done(((f32[8,2,2176]{2,1,0:T(2,128)}), f32[8,2,2176]{2,1,0:T(2,128)S(1)}, u32[]{:S(2)}, u32[]{:S(2)}) %all-to-all-start.1) | async-done | bytes 139296 | tf_op jit(solution)/shard_map/all_to_all | solution.py:116
  103.0 0.2 fusion.34
  103.4 0.2 convolution_bitcast_fusion
  103.8 8.1 %all-gather.1 = f32[4,2,256]{2,1,0:T(2,128)S(1)} all-gather(f32[1,2,256]{2,1,0:T(2,128)S(1)} %maximum_bitcast_fusion.2), channel_id=2, replica_groups=mesh['sp'=4,'tp'=8] {'sp'}, dimensions={0}, use_global_device_ids=true | all-gather | bytes 10240 | tf_op jit(solution)/shard_map/all_gather | solution.py:156
  112.6 0.6 broadcast_in_dim.37
  113.2 3.3 %all-to-all-start.2 = ((f32[8,2,2,256]{3,2,1,0:T(2,128)}), f32[8,2,2,256]{3,2,1,0:T(2,128)S(1)}, u32[]{:S(2)}, u32[]{:S(2)}) async-start(f32[8,2,2,256]{3,2,1,0:T(2,128)} %broadcast_in_dim.37), calls=%async_computation.2 | async-start | bytes 65536 | tf_op jit(solution)/shard_map/all_to_all | solution.py:161
  116.5 28.0 %all-gather.7.cloned.1.call-done = bf16[16384,128]{1,0:T(8,128)(2,1)} async-done(((bf16[512,128]{1,0:T(8,128)(2,1)}), bf16[16384,128]{1,0:T(8,128)(2,1)}) %all-gather.7.cloned.1.call-update) | async-done | bytes 4194320 | tf_op jit(solution)/shard_map/all_gather | solution.py:28
  144.6 6.2 %project_blocks.3 = bf16[512,1024]{1,0:T(8,128)(2,1)} custom-call(bf16[512,2048]{1,0:T(8,128)(2,1)} %bitcast.104, bf16[4,8,512,128]{3,2,1,0:T(8,128)(2,1)} %bitcast.115), custom_call_target="tpu_custom_call" | custom-call | flops 2147483648 | bytes 7340032 | tf_op jit(solution)/shard_map/project_blocks/pallas_call | solution.py:47
  151.8 0.6 fusion.23
  (64 shorter events, 3.1 us)
Async XLA Ops:
  7.2 1.8 %copy-start = (bf16[2048,128]{1,0:T(8,128)(2,1)S(1)}, bf16[2048,128]{1,0:T(8,128)(2,1)}, u32[]{:S(2)}) copy-start(bf16[2048,128]{1,0:T(8,128)(2,1)} %param.11) | copy-start | bytes 1572868
  7.2 72.6 %all-gather.5.cloned.1.call-start = ((), (), s32[]{:S(2)}) async-start(), calls=%async_computation.3 | async-start | bytes 4325376 | tf_op jit(solution)/shard_map/all_gather | solution.py:28
  8.9 135.7 %all-gather.7.cloned.1.call-start = ((), (), s32[]{:S(2)}) async-start(), calls=%async_computation.4 | async-start | bytes 4325376 | tf_op jit(solution)/shard_map/all_gather | solution.py:28
  9.6 5.4 %copy-start.2 = (bf16[2048,128]{1,0:T(8,128)(2,1)S(1)}, bf16[2048,128]{1,0:T(8,128)(2,1)}, u32[]{:S(2)}) copy-start(bf16[2048,128]{1,0:T(8,128)(2,1)} %param.10) | copy-start | bytes 1572868
  9.6 5.4 %copy-start.3 = (bf16[2,2048]{1,0:T(2,128)(2,1)S(1)}, bf16[2,2048]{1,0:T(2,128)(2,1)}, u32[]{:S(2)}) copy-start(bf16[2,2048]{1,0:T(2,128)(2,1)} %param.8) | copy-start | bytes 24580
  9.7 31.1 %all-to-all-start = ((bf16[4,128,2048]{2,1,0:T(8,128)(2,1)}), bf16[4,128,2048]{2,1,0:T(8,128)(2,1)S(1)}, u32[]{:S(2)}, u32[]{:S(2)}) async-start(bf16[4,128,2048]{2,1,0:T(8,128)(2,1)} %bitcast.105), calls=%async_computation | async-start | bytes 4194304 | tf_op jit(solution)/shard_map/all_to_all | solution.py:139
  40.8 39.0 %copy-start.1 = (bf16[4,128,2048]{2,1,0:T(8,128)(2,1)}, bf16[4,128,2048]{2,1,0:T(8,128)(2,1)S(1)}, u32[]{:S(2)}) copy-start(bf16[4,128,2048]{2,1,0:T(8,128)(2,1)S(1)} %all-to-all-done) | copy-start | bytes 6291460
  87.7 6.9 %copy-start.4 = (f32[8]{0:T(128)S(1)}, f32[8]{0:T(128)}, u32[]{:S(2)}) copy-start(f32[8]{0:T(128)} %param.12) | copy-start | bytes 100
  87.7 6.9 %copy-start.5 = (f32[128]{0:T(128)S(1)}, f32[128]{0:T(128)}, u32[]{:S(2)}) copy-start(f32[128]{0:T(128)} %param.13) | copy-start | bytes 1540
  91.0 11.5 %all-to-all-start.1 = ((f32[8,2,2176]{2,1,0:T(2,128)}), f32[8,2,2176]{2,1,0:T(2,128)S(1)}, u32[]{:S(2)}, u32[]{:S(2)}) async-start(f32[8,2,2176]{2,1,0:T(2,128)} %reshape_reshape.3), calls=%async_computation.1 | async-start | bytes 278528 | tf_op jit(solution)/shard_map/all_to_all | solution.py:116
  113.2 37.6 %all-to-all-start.2 = ((f32[8,2,2,256]{3,2,1,0:T(2,128)}), f32[8,2,2,256]{3,2,1,0:T(2,128)S(1)}, u32[]{:S(2)}, u32[]{:S(2)}) async-start(f32[8,2,2,256]{3,2,1,0:T(2,128)} %broadcast_in_dim.37), calls=%async_computation.2 | async-start | bytes 65536 | tf_op jit(solution)/shard_map/all_to_all | solution.py:161
Sparse Core Ops, SparseCore 0:
  11.6 68.1 all-gather.4
  82.8 61.6 all-gather.6
